TPU v7x, 32 devices: a whole 2x2x4 slice. The times are simulated.
32 devices in a mesh: fs: 16 (over z, y, x), tp: 2 (over core).
Axes of the slice: x: 2, y: 2, z: 4, core: 2. Of those that a mesh axis runs over, the one named last changes fastest.
Arguments:
- saved_inputs: bfloat16 [12288, 2048], P('fs'), may hold values from -8 to 8
- input_cot: bfloat16 [12288, 2048], P('fs', 'tp'), may hold values from -0.0546875 to 0.0546875
- gate_cot: bfloat16 [12288, 2048], P('fs', 'tp'), may hold values from -0.0546875 to 0.0546875
- input_master: float32 [2048, 2048], P('fs', 'tp'), may hold values from -6 to 6
- gate_master: float32 [2048, 2048], P('fs', 'tp'), may hold values from -6 to 6
- input_factor: bfloat16 [2048, 256], P('fs'), may hold values from -2 to 2
- gate_factor: bfloat16 [2048, 256], P('fs'), may hold values from -2 to 2
- input_first: float32 [256, 2048], P('fs', 'tp'), may hold values from -6 to 6
- input_second: float32 [256, 2048], P('fs', 'tp'), may hold values from 0.2 to 17
- gate_first: float32 [256, 2048], P('fs', 'tp'), may hold values from -6 to 6
- gate_second: float32 [256, 2048], P('fs', 'tp'), may hold values from 0.2 to 17
Outputs:
- input_step: float32 [2048, 2048], P('fs', 'tp')
- gate_step: float32 [2048, 2048], P('fs', 'tp')
- input_first_new: float32 [256, 2048], P('fs', 'tp')
- input_second_new: float32 [256, 2048], P('fs', 'tp')
- gate_first_new: float32 [256, 2048], P('fs', 'tp')
- gate_second_new: float32 [256, 2048], P('fs', 'tp')
- input_copy: bfloat16 [2048, 2048], P(None, 'tp')
- gate_copy: bfloat16 [2048, 2048], P(None, 'tp')
All inputs are finite; a program needn't handle non-finite values.
Results may differ from a plain program's by a relative error of at most 0.0004.
Values may be sent and summed in bfloat16 or wider, within the bound.
A program may use at most 64 MiB of HBM per device.

v0:
```python
import functools

import jax
import jax.numpy as jnp
from jax import lax
from jax.experimental import pallas as pl
from jax.experimental.pallas import tpu as pltpu
from jax.sharding import PartitionSpec as P

first_decay = 0.9
second_decay = 0.9
ratio_floor = 1e-08
mean_floor = 1e-06
step_size = 0.05
PLANE = 4
VMEM = pltpu.VMEM
DMA = pltpu.SemaphoreType.DMA
MESH = pl.DeviceIdType.MESH


class Place:
    def __init__(self, n):
        self.n = n
        self.depth = n // PLANE
        self.f = lax.axis_index("fs")
        self.z = lax.div(self.f, PLANE)
        self.spot = lax.rem(self.f, PLANE)
        self.x = lax.rem(self.f, 2)
        self.y = lax.div(self.spot, 2)
        self.fx = self.f + 1 - 2 * self.x
        self.fy = self.f + 2 - 4 * self.y
        self.sx = self.spot + 1 - 2 * self.x
        self.sy = self.spot + 2 - 4 * self.y

    def twin(self, s):
        other = self.z
        bit = 1
        while bit <= s:
            if s // bit % 2:
                other = other + bit - 2 * bit * lax.rem(lax.div(self.z, bit), 2)
            bit *= 2
        return other


def send(src, dst, s_sem, r_sem, axis, target):
    return pltpu.make_async_remote_copy(
        src_ref=src,
        dst_ref=dst,
        send_sem=s_sem,
        recv_sem=r_sem,
        device_id={axis: target},
        device_id_type=MESH,
    )


def greet(targets):
    barrier = pltpu.get_barrier_semaphore()
    for axis, target in targets:
        pl.semaphore_signal(barrier, inc=1, device_id={axis: target}, device_id_type=MESH)
    pl.semaphore_wait(barrier, len(targets))


def whole_block(ref, index):
    return ref.at[index]


def gather(at, a, b, s_z, r_z, s_p, r_p, view=whole_block, arrived=None):
    depth = at.depth
    started = []

    def go(ref, index, s_sem, r_sem, target):
        copy = send(view(ref, index), view(ref, index), s_sem, r_sem, "fs", target)
        copy.start()
        started.append(copy)
        return copy

    far = [None]

    def reach(dz):
        target = at.twin(dz) * PLANE + at.spot
        far.append(
            (
                go(a, at.f, s_z.at[dz, 0], r_z.at[dz, 0], target),
                go(b, at.f, s_z.at[dz, 1], r_z.at[dz, 1], target),
            )
        )

    near = []
    for s in range(depth):
        base = at.twin(s) * PLANE
        mine = base + at.spot
        if s > 0:
            far[s][0].wait_recv()
        xa = go(a, mine, s_p.at[s, 0], r_p.at[s, 0], at.fx)
        ya = go(a, mine, s_p.at[s, 1], r_p.at[s, 1], at.fy)
        if s > 0:
            far[s][1].wait_recv()
        yb = go(b, mine, s_p.at[s, 2], r_p.at[s, 2], at.fy)
        xb = go(b, mine, s_p.at[s, 3], r_p.at[s, 3], at.fx)
        if s == 0:
            for dz in range(1, depth):
                reach(dz)
        if s == 1:
            near[0][3].wait_recv()
            near[0][4].wait_recv()
            corner = at.z * PLANE + PLANE - 1 - at.spot
            target = at.twin(1) * PLANE + at.spot
            ca = go(a, corner, s_p.at[s, 4], r_p.at[s, 4], target)
            cb = go(b, corner, s_p.at[s, 5], r_p.at[s, 5], target)
            near[0] = near[0][:3]
            near.append((base, xa, ya, yb, xb, ca, cb))
            continue
        xa.wait_recv()
        ra = go(a, base + at.sx, s_p.at[s, 4], r_p.at[s, 4], at.fy)
        yb.wait_recv()
        rb = go(b, base + at.sy, s_p.at[s, 5], r_p.at[s, 5], at.fx)
        near.append((base, ya, xb, ra, rb))
    for base, *group in near:
        for copy in group:
            copy.wait_recv()
        if arrived is not None:
            arrived(base)
    for copy in started:
        copy.wait_send()


def gather_sems(n):
    depth = n // PLANE
    return [DMA((depth, 2)), DMA((depth, 2)), DMA((depth, 6)), DMA((depth, 6))]


def moments(low_rank, first, second):
    first_new = first_decay * first + (1.0 - first_decay) * low_rank
    second_new = second_decay * second + (1.0 - second_decay) * low_rank * low_rank
    ratio = first_new / (jnp.sqrt(second_new) + ratio_floor)
    return (first_new, second_new, ratio)


def wide_dot(narrow, wide):
    total = None
    rest = wide
    for _ in range(3):
        part = rest.astype(jnp.bfloat16)
        rest = rest - part.astype(jnp.float32)
        term = jnp.dot(narrow, part, preferred_element_type=jnp.float32)
        total = term if total is None else total + term
    return total


def main_kernel(
    n,
    m,
    saved_hbm,
    cot_a_hbm,
    cot_b_hbm,
    master_a_hbm,
    master_b_hbm,
    factor_a,
    factor_b,
    first_a,
    second_a,
    first_b,
    second_b,
    step_a,
    step_b,
    first_a_new,
    second_a_new,
    first_b_new,
    second_b_new,
    copy_a_hbm,
    copy_b_hbm,
    saved,
    cot_a,
    cot_b,
    master_a,
    master_b,
    whole_a,
    whole_b,
    mid_a,
    mid_b,
    term_a,
    term_b,
    copy_a,
    copy_b,
    one_a,
    one_b,
    two_a,
    two_b,
    sum_a,
    sum_b,
    ready_a,
    ready_b,
    far_a,
    far_b,
    all_a,
    all_b,
    pair,
    total,
    load_sem,
    store_sem,
    s_mate,
    r_mate,
    s_one,
    r_one,
    s_two,
    r_two,
    s_far,
    r_far,
    fz_s,
    fz_r,
    fp_s,
    fp_r,
    rz_s,
    rz_r,
    rp_s,
    rp_r,
    s_tp,
    r_tp,
    s_fs,
    r_fs,
    cz_s,
    cz_r,
    cp_s,
    cp_r,
):
    at = Place(n)
    depth = at.depth
    t = lax.axis_index("tp")
    others = [lax.rem(at.f + k, n) for k in range(1, n)]
    mates = [lax.rem(t + k, m) for k in range(1, m)]
    loads = [
        pltpu.make_async_copy(src, dst, load_sem.at[k])
        for k, (src, dst) in enumerate(
            (
                (saved_hbm, saved),
                (cot_a_hbm, cot_a),
                (cot_b_hbm, cot_b),
                (master_a_hbm, master_a),
                (master_b_hbm, master_b),
            )
        )
    ]
    for load in loads:
        load.start()
    whole_a[at.f] = factor_a[...]
    whole_b[at.f] = factor_b[...]
    greet([("fs", o) for o in others] + [("tp", o) for o in mates])
    started = []

    def go(copy):
        copy.start()
        started.append(copy)
        return copy

    rows = factor_a.shape[0]
    parts = 2 if m % 2 == 0 else 1
    mate = t + 1 - 2 * lax.rem(t, 2)
    half = pl.ds(pl.multiple_of(lax.rem(t, 2) * (rows // 2), rows // 2), rows // 2) if parts == 2 else pl.ds(0, rows)
    passed = []
    width = PLANE * rows

    def multiply(k):
        base, copies = passed[k]
        for copy in copies:
            copy.wait_recv()
        if k == 0:
            loads[0].wait()
        columns = pl.ds(pl.multiple_of(base * rows, width), width)
        for mid, whole in ((mid_a, whole_a), (mid_b, whole_b)):
            block = whole[pl.ds(base, PLANE)].reshape(width, whole.shape[2])
            product = jnp.dot(saved[:, columns], block, preferred_element_type=jnp.float32)
            if k == 0:
                mid[...] = product
            else:
                mid[...] += product

    def arrived(base):
        k = len(passed)
        copies = []
        if parts == 2:
            for side, whole in enumerate((whole_a, whole_b)):
                view = whole.at[pl.ds(base, PLANE), half]
                copies.append(go(send(view, view, s_mate.at[k, side], r_mate.at[k, side], "tp", mate)))
        passed.append((base, copies))
        if k > 0:
            multiply(k - 1)

    gather(at, whole_a, whole_b, fz_s, fz_r, fp_s, fp_r, lambda ref, index: ref.at[index, half], arrived)
    multiply(depth - 1)

    def project(mid, cot):
        rest = mid[...].T
        result = None
        for _ in range(3):
            part = rest.astype(jnp.bfloat16)
            rest = rest - part.astype(jnp.float32)
            piece = jnp.dot(part, cot[...], preferred_element_type=jnp.float32)
            result = piece if result is None else result + piece
        return result

    loads[1].wait()
    term_a[...] = project(mid_a, cot_a).reshape(term_a.shape)
    first_a_stage = []
    for k in range(depth):
        plane = at.twin(depth - 1 - k)
        first_a_stage.append(
            go(send(term_a.at[plane, :, 1 - at.x], one_a.at[k], s_one.at[k, 0], r_one.at[k, 0], "fs", at.fx))
        )
    loads[2].wait()
    term_b[...] = project(mid_b, cot_b).reshape(term_b.shape)
    first_stage = []
    for k in range(depth):
        plane = at.twin(depth - 1 - k)
        pair_b = go(send(term_b.at[plane, 1 - at.y], one_b.at[k], s_one.at[k, 1], r_one.at[k, 1], "fs", at.fy))
        first_stage.append((first_a_stage[k], pair_b))
    second_stage = []
    third_stage = []
    for k in range(depth + 1):
        if k < depth:
            plane = at.twin(depth - 1 - k)
            first_stage[k][0].wait_recv()
            sum_a[k] = term_a[plane, :, at.x] + one_a[k]
            ca = go(send(sum_a.at[k, 1 - at.y], two_a.at[k], s_two.at[k, 0], r_two.at[k, 0], "fs", at.fy))
            first_stage[k][1].wait_recv()
            sum_b[k] = term_b[plane, at.y] + one_b[k]
            cb = go(send(sum_b.at[k, 1 - at.x], two_b.at[k], s_two.at[k, 1], r_two.at[k, 1], "fs", at.fx))
            second_stage.append((ca, cb))
        if k > 0:
            j = k - 1
            target = at.twin(depth - k) * PLANE + at.spot
            second_stage[j][0].wait_recv()
            ready_a[j] = sum_a[j, at.y] + two_a[j]
            if j < depth - 1:
                ca = go(send(ready_a.at[j], far_a.at[j], s_far.at[j, 0], r_far.at[j, 0], "fs", target))
            second_stage[j][1].wait_recv()
            ready_b[j] = sum_b[j, at.x] + two_b[j]
            if j < depth - 1:
                cb = go(send(ready_b.at[j], far_b.at[j], s_far.at[j, 1], r_far.at[j, 1], "fs", target))
                third_stage.append((ca, cb))
    low_a = ready_a[depth - 1]
    low_b = ready_b[depth - 1]
    for j in range(depth - 1):
        third_stage[j][0].wait_recv()
        low_a = low_a + far_a[j]
        third_stage[j][1].wait_recv()
        low_b = low_b + far_b[j]

    new_first, new_second, ratio = moments(low_a, first_a[...], second_a[...])
    first_a_new[...] = new_first
    second_a_new[...] = new_second
    all_a[at.f] = ratio
    new_first, new_second, ratio = moments(low_b, first_b[...], second_b[...])
    first_b_new[...] = new_first
    second_b_new[...] = new_second
    all_b[at.f] = ratio

    gather(at, all_a, all_b, rz_s, rz_r, rp_s, rp_r)

    rank = all_a.shape[0] * all_a.shape[1]
    cols = all_a.shape[2]
    dir_a = wide_dot(factor_a[...], all_a[...].reshape(rank, cols))
    dir_b = wide_dot(factor_b[...], all_b[...].reshape(rank, cols))
    count = n * dir_a.shape[0] * m * cols

    pair[0, 0:8] = jnp.full((8, 128), jnp.sum(dir_a * dir_a), jnp.float32)
    pair[0, 8:16] = jnp.full((8, 128), jnp.sum(dir_b * dir_b), jnp.float32)
    trips = [
        go(send(pair.at[0], pair.at[k + 1], s_tp.at[k], r_tp.at[k], "tp", mate)) for k, mate in enumerate(mates)
    ]
    step_a[...] = dir_a
    step_b[...] = dir_b
    joint = pair[0]
    for k, trip in enumerate(trips):
        trip.wait_recv()
        joint = joint + pair[k + 1]
    total[0] = joint
    trips = [
        go(send(total.at[0], total.at[k + 1], s_fs.at[k], r_fs.at[k], "fs", other)) for k, other in enumerate(others)
    ]
    joint = total[0]
    for k, trip in enumerate(trips):
        trip.wait_recv()
        joint = joint + total[k + 1]
    scale = lax.rsqrt(joint / count + mean_floor)
    new_step = step_a[...] * scale[0:1, 0:1]
    step_a[...] = new_step
    loads[3].wait()
    copy_a[at.f] = (master_a[...] - step_size * new_step).astype(jnp.bfloat16)
    new_step = step_b[...] * scale[8:9, 0:1]
    step_b[...] = new_step
    loads[4].wait()
    copy_b[at.f] = (master_b[...] - step_size * new_step).astype(jnp.bfloat16)

    stores = []

    def put(base):
        k = len(stores)
        block = pl.ds(base, PLANE)
        for side, (src, dst) in enumerate(((copy_a, copy_a_hbm), (copy_b, copy_b_hbm))):
            stores.append(pltpu.make_async_copy(src.at[block], dst.at[block], store_sem.at[k + side]))
            stores[-1].start()

    gather(at, copy_a, copy_b, cz_s, cz_r, cp_s, cp_r, whole_block, put)
    for store in stores:
        store.wait()
    for copy in started:
        copy.wait_send()


def hand_kernel(depth, *refs):
    count = (len(refs) - 2) // 3
    given, out, held = refs[:count], refs[count : 2 * count], refs[2 * count : 3 * count]
    in_sem, out_sem = refs[3 * count :]
    moves = []
    for k in range(count):
        pieces = depth if len(given[k].shape) == 3 else 1
        size = given[k].shape[0] // pieces
        for i in range(pieces):
            part = pl.ds(i * size, size)
            moves.append(
                (
                    pltpu.make_async_copy(given[k].at[part], held[k].at[part], in_sem.at[k, i]),
                    pltpu.make_async_copy(held[k].at[part], out[k].at[part], out_sem.at[k, i]),
                )
            )
    for into, _ in moves:
        into.start()
    for into, onward in moves:
        into.wait()
        onward.start()
    for _, onward in moves:
        onward.wait()


def local(
    n,
    m,
    saved_inputs,
    input_cot,
    gate_cot,
    input_master,
    gate_master,
    input_factor,
    gate_factor,
    input_first,
    input_second,
    gate_first,
    gate_second,
):
    in_vmem = pl.BlockSpec(memory_space=VMEM)
    anywhere = pl.BlockSpec(memory_space=pl.ANY)
    rows, rank = input_factor.shape
    tokens = saved_inputs.shape[0]
    low_rows, cols = input_first.shape
    depth = n // PLANE
    shape = jax.ShapeDtypeStruct
    f32, bf16 = jnp.float32, jnp.bfloat16
    low = shape((low_rows, cols), f32)
    piece = (low_rows, cols)
    full = shape((rows, cols), f32)
    copies = shape((n, rows, cols), bf16)
    shapes = [full, full, low, low, low, low, copies, copies]
    outs = pl.pallas_call(
        functools.partial(main_kernel, n, m),
        out_shape=shapes,
        in_specs=[anywhere] * 5 + [in_vmem] * 6,
        out_specs=[in_vmem] * 6 + [anywhere] * 2,
        scratch_shapes=[
            VMEM(saved_inputs.shape, bf16),
            VMEM(input_cot.shape, bf16),
            VMEM(input_cot.shape, bf16),
            VMEM((rows, cols), f32),
            VMEM((rows, cols), f32),
            VMEM((n, rows, rank), bf16),
            VMEM((n, rows, rank), bf16),
            VMEM((tokens, rank), f32),
            VMEM((tokens, rank), f32),
            VMEM((depth, 2, 2) + piece, f32),
            VMEM((depth, 2, 2) + piece, f32),
            VMEM((n, rows, cols), bf16),
            VMEM((n, rows, cols), bf16),
            VMEM((depth, 2) + piece, f32),
            VMEM((depth, 2) + piece, f32),
            VMEM((depth,) + piece, f32),
            VMEM((depth,) + piece, f32),
            VMEM((depth, 2) + piece, f32),
            VMEM((depth, 2) + piece, f32),
            VMEM((depth,) + piece, f32),
            VMEM((depth,) + piece, f32),
            VMEM((depth,) + piece, f32),
            VMEM((depth,) + piece, f32),
            VMEM((n,) + piece, f32),
            VMEM((n,) + piece, f32),
            VMEM((m, 16, 128), f32),
            VMEM((n, 16, 128), f32),
            DMA((5,)),
            DMA((2 * depth,)),
            *[DMA((depth, 2))] * 8,
            *gather_sems(n),
            *gather_sems(n),
            DMA((m,)),
            DMA((m,)),
            DMA((n,)),
            DMA((n,)),
            *gather_sems(n),
        ],
        compiler_params=pltpu.CompilerParams(
            collective_id=1, has_side_effects=True, vmem_limit_bytes=56 * 2**20
        ),
        name="update",
    )(
        saved_inputs,
        input_cot,
        gate_cot,
        input_master,
        gate_master,
        input_factor,
        gate_factor,
        input_first,
        input_second,
        gate_first,
        gate_second,
    )
    outs = pl.pallas_call(
        functools.partial(hand_kernel, depth),
        out_shape=shapes,
        in_specs=[anywhere] * 8,
        out_specs=[anywhere] * 8,
        scratch_shapes=[VMEM(s.shape, s.dtype) for s in shapes] + [DMA((8, depth))] * 2,
        name="results",
    )(*outs)
    *head, copy_in, copy_gate = outs
    return (*head, copy_in.reshape(n * rows, cols), copy_gate.reshape(n * rows, cols))


def solution(mesh):
    n, m = mesh.shape["fs"], mesh.shape["tp"]
    both = P("fs", "tp")
    rows = P("fs", None)
    return jax.shard_map(
        functools.partial(local, n, m),
        mesh=mesh,
        in_specs=(rows, both, both, both, both, rows, rows, both, both, both, both),
        out_specs=(both,) * 6 + (P(None, "tp"),) * 2,
        check_vma=False,
    )
```

profile of v0, /device:TPU:0, one launch (start us, length us, event | category | flops | bytes accessed | tf_op | source)
XLA Modules:
  0.0 167.1 jit_solution(11092235093708117870)
XLA Ops:
  0.6 158.4 %update.1 = (f32[128,1024]{1,0:T(8,128)}, f32[128,1024]{1,0:T(8,128)}, f32[16,1024]{1,0:T(8,128)}, f32[16,1024]{1,0:T(8,128)}, f32[16,1024]{1,0:T(8,128)}, /*ind...) custom-call(bf16[768,2048]{1,0:T(8,128)(2,1)} %saved_hbm.1, ...), custom_call_target="tpu_custom_call" | custom-call | tf_op jit(solution)/shard_map/update/pallas_call | solution.py:463
  159.0 8.1 %results.1 = (f32[128,1024]{1,0:T(8,128)}, f32[128,1024]{1,0:T(8,128)}, f32[16,1024]{1,0:T(8,128)}, f32[16,1024]{1,0:T(8,128)}, f32[16,1024]{1,0:T(8,128)}, /*in...) custom-call(f32[128,1024]{1,0:T(8,128)} %get-tuple-element.24.refs_0_, ...), custom_call_target="tpu_custom_call" | custom-call | tf_op jit(solution)/shard_map/results/pallas_call | solution.py:524
where the time goes:
time: 167 us
  Pallas kernels  166 us (99%)
    pallas_call x1, Pallas kernels, local(): pl.pallas_call(functools.partial(main_kernel, n, m), out_shape=shapes, in...  158 us
    pallas_call x1, Pallas kernels, local(): pl.pallas_call(functools.partial(hand_kernel, depth), out_shape=shapes, i...  8.11 us

commit v1 on v0

v1 whole, which is shorter than its diff:
```python
import functools

import jax
import jax.numpy as jnp
from jax import lax
from jax.experimental import pallas as pl
from jax.experimental.pallas import tpu as pltpu
from jax.sharding import PartitionSpec as P

first_decay = 0.9
second_decay = 0.9
ratio_floor = 1e-08
mean_floor = 1e-06
step_size = 0.05
PLANE = 4
HOP = 2.0
RATE = 46600.0
VMEM = pltpu.VMEM
DMA = pltpu.SemaphoreType.DMA
MESH = pl.DeviceIdType.MESH


class Place:
    def __init__(self, n):
        self.n = n
        self.depth = n // PLANE
        self.f = lax.axis_index("fs")
        self.z = lax.div(self.f, PLANE)
        self.spot = lax.rem(self.f, PLANE)
        self.x = lax.rem(self.f, 2)
        self.y = lax.div(self.spot, 2)
        self.fx = self.f + 1 - 2 * self.x
        self.fy = self.f + 2 - 4 * self.y
        self.sx = self.spot + 1 - 2 * self.x
        self.sy = self.spot + 2 - 4 * self.y

    def twin(self, s):
        other = self.z
        bit = 1
        while bit <= s:
            if s // bit % 2:
                other = other + bit - 2 * bit * lax.rem(lax.div(self.z, bit), 2)
            bit *= 2
        return other

    def column(self, s):
        return self.twin(s) * PLANE + self.spot


def send(src, dst, s_sem, r_sem, axis, target):
    return pltpu.make_async_remote_copy(
        src_ref=src,
        dst_ref=dst,
        send_sem=s_sem,
        recv_sem=r_sem,
        device_id={axis: target},
        device_id_type=MESH,
    )


def greet(targets):
    barrier = pltpu.get_barrier_semaphore()
    for axis, target in targets:
        pl.semaphore_signal(barrier, inc=1, device_id={axis: target}, device_id_type=MESH)
    pl.semaphore_wait(barrier, len(targets))


def merge(streams):
    heads = [[next(g, None), g] for g in streams]
    while True:
        live = [head for head in heads if head[0] is not None]
        if not live:
            return
        head = min(live, key=lambda h: h[0])
        head[0] = next(head[1], None)


def in_order(events):
    for when, act in sorted(events, key=lambda e: e[0]):
        yield when
        act()


def gather(at, go, view, sems, start, unit, arrived=None):
    s_z, r_z, s_p, r_p = sems
    depth = at.depth
    far, near = {}, {}
    waited = set()

    def hop(half, index, s_sem, r_sem, target):
        ref = view(half, index)
        return go(send(ref, ref, s_sem, r_sem, "fs", target))

    def need(copy):
        if id(copy) not in waited:
            waited.add(id(copy))
            copy.wait_recv()

    def reach():
        for s in range(1, depth):
            far[s] = [hop(h, at.f, s_z.at[s, h], r_z.at[s, h], at.column(s)) for h in range(2)]

    def issue(s):
        mine = at.column(s)
        got = near[s] = {}

        def x(h, k):
            got[k] = hop(h, mine, s_p.at[s, k], r_p.at[s, k], at.fx)

        def y(h, k):
            got[k] = hop(h, mine, s_p.at[s, k], r_p.at[s, k], at.fy)

        if s == 0:
            x(0, 0), y(1, 2), y(0, 1), x(1, 3)
            reach()
        else:
            need(far[s][0])
            x(0, 0), y(0, 1)
            need(far[s][1])
            y(1, 2), x(1, 3)

    def relay(s):
        base = at.twin(s) * PLANE
        need(near[s][0])
        near[s][4] = hop(0, base + at.sx, s_p.at[s, 4], r_p.at[s, 4], at.fy)
        need(near[s][2])
        near[s][5] = hop(1, base + at.sy, s_p.at[s, 5], r_p.at[s, 5], at.fx)

    def corner(s):
        index = at.twin(s) * PLANE + PLANE - 1 - at.spot
        for h in range(2):
            need(near[s][4 + h])
            near[s + 1][4 + h] = hop(h, index, s_p.at[s + 1, 4 + h], r_p.at[s + 1, 4 + h], at.column(1))

    def done(s):
        for k in sorted(near[s]):
            need(near[s][k])
        if arrived is not None:
            arrived(at.twin(s) * PLANE)

    events = []
    free = start
    cornered = start
    for s in range(depth):
        when = free if s == 0 else max(free, start + 2 * unit * s + HOP)
        events.append((when, functools.partial(issue, s)))
        if s % 2 == 0:
            free = when + 3 * unit
            cornered = when + 3 * unit + 2 * HOP
            events.append((when + unit + HOP, functools.partial(relay, s)))
            if s + 1 < depth:
                events.append((max(cornered, free + 0.01), functools.partial(corner, s)))
            events.append((cornered + 0.02, functools.partial(done, s)))
        else:
            free = when + 2 * unit
            cornered = max(cornered, free) + 2 * unit + HOP
            events.append((cornered + 0.02, functools.partial(done, s)))
    times = {}
    for k, (when, act) in enumerate(events):
        if act.func is issue:
            times[act.args[0]] = when
    fixed = []
    for when, act in events:
        if act.func is corner:
            when = max(when, times[act.args[0] + 1] + 0.01)
        fixed.append((when, act))
    yield from in_order(fixed)


def gather_sems(n, copies=None):
    depth = n // PLANE
    lead = () if copies is None else (copies,)
    return [DMA(lead + (depth, 2)), DMA(lead + (depth, 2)), DMA(lead + (depth, 6)), DMA(lead + (depth, 6))]


def moments(low_rank, first, second):
    first_new = first_decay * first + (1.0 - first_decay) * low_rank
    second_new = second_decay * second + (1.0 - second_decay) * low_rank * low_rank
    ratio = first_new / (jnp.sqrt(second_new) + ratio_floor)
    return (first_new, second_new, ratio)


def split(wide):
    parts = []
    for _ in range(3):
        part = wide.astype(jnp.bfloat16)
        wide = wide - part.astype(jnp.float32)
        parts.append(part)
    return parts


def dot(left, right):
    return jnp.dot(left, right, preferred_element_type=jnp.float32)


def main_kernel(n, m, *refs):
    (
        saved_hbm, cot_a_hbm, cot_b_hbm, master_a_hbm, master_b_hbm, factor_a_hbm, factor_b_hbm,
        first_a_hbm, second_a_hbm, first_b_hbm, second_b_hbm,
        step, first_out, second_out, copies,
        saved, cot, master, left, first, second, whole, mid, term,
        one, total, two, ready, far, ratios, pair,
        load_sem, s_mate, r_mate, s_one, r_one, s_two, r_two, s_far, r_far, s_tp, r_tp,
        *rest,
    ) = refs
    factor_sems, ratio_sems, copy_sems = rest[0:4], rest[4:8], rest[8:12]
    at = Place(n)
    depth = at.depth
    t = lax.axis_index("tp")
    own = lax.rem(t, 2) if m % 2 == 0 else 0
    mate = t + 1 - 2 * own
    mates = [lax.rem(t + k, m) for k in range(1, m)]
    rows, rank = factor_a_hbm.shape
    low_rows, cols = first_a_hbm.shape
    half = cols // 2
    width = PLANE * rows

    def load(k, src, dst):
        copy = pltpu.make_async_copy(src, dst, load_sem.at[k])
        copy.start()
        return copy

    top = pl.ds(0, rows)
    gram = pl.ds(rows, 3 * rank)
    factor_loads = [load(0, factor_a_hbm, left.at[0, top]), load(1, factor_b_hbm, left.at[1, top])]
    saved_load = load(2, saved_hbm, saved)
    cot_loads = [load(3, cot_a_hbm, cot.at[0]), load(4, cot_b_hbm, cot.at[1])]
    other_loads = [
        load(5 + k, src, dst)
        for k, (src, dst) in enumerate(
            (
                (first_a_hbm, first.at[0]),
                (second_a_hbm, second.at[0]),
                (first_b_hbm, first.at[1]),
                (second_b_hbm, second.at[1]),
                (master_a_hbm, master.at[0]),
                (master_b_hbm, master.at[1]),
            )
        )
    ]
    greet([("fs", at.fx), ("fs", at.fy)] + [("fs", at.column(s)) for s in range(1, depth)] + [("tp", o) for o in mates])
    started = []

    def go(copy):
        copy.start()
        started.append(copy)
        return copy

    for copy in factor_loads:
        copy.wait()

    def factor_gather(j, i, start):
        multiplied = []
        whole[at.f] = left[i, 0:rows]

        def arrived(base):
            if not multiplied:
                if j == 0:
                    saved_load.wait()
            columns = pl.ds(pl.multiple_of(base * rows, width), width)
            product = dot(saved[:, columns], whole[pl.ds(base, PLANE)].reshape(width, rank))
            if multiplied:
                mid[i] += product
            else:
                mid[i] = product
            multiplied.append(base)

        size = rows // 2
        yield from gather(
            at,
            go,
            lambda h, index: whole.at[index, pl.ds(h * size, size)],
            factor_sems,
            start,
            size * rank * 2 / RATE,
            arrived,
        )

    def find_gram(i):
        factor = whole[...].reshape(n * rows, rank)
        product = lax.dot_general(factor, factor, (((0,), (0,)), ((), ())), preferred_element_type=jnp.float32)
        for k, part in enumerate(split(product)):
            left[i, rows + k * rank : rows + (k + 1) * rank] = part

    merge([factor_gather(0, own, 0.0)])
    mid_trip = go(send(mid.at[own], mid.at[own], s_mate.at[0], r_mate.at[0], "tp", mate))
    gram_trip = []

    def project(j, i):
        result = None
        for part in split(mid[i].T):
            piece = dot(part, cot[i])
            result = piece if result is None else result + piece
        for h in range(2):
            term[j, h] = result[:, h * half : (h + 1) * half].reshape(depth, 2, 2, low_rows, half)

    def reduce_scatter(j, i, start, after_first):
        unit = 2 * low_rows * half * 4 / RATE
        first_stage, second_stage, third_stage = {}, {}, {}

        def stage_one(k):
            plane = at.twin(depth - 1 - k)
            first_stage[k] = (
                go(send(term.at[j, 0, plane, :, 1 - at.x], one.at[j, 0, k], s_one.at[j, k, 0], r_one.at[j, k, 0], "fs", at.fx)),
                go(send(term.at[j, 1, plane, 1 - at.y], one.at[j, 1, k], s_one.at[j, k, 1], r_one.at[j, k, 1], "fs", at.fy)),
            )

        def stage_two(k):
            plane = at.twin(depth - 1 - k)
            first_stage[k][0].wait_recv()
            total[j, 0, k] = term[j, 0, plane, :, at.x] + one[j, 0, k]
            a = go(send(total.at[j, 0, k, 1 - at.y], two.at[j, 0, k], s_two.at[j, k, 0], r_two.at[j, k, 0], "fs", at.fy))
            first_stage[k][1].wait_recv()
            total[j, 1, k] = term[j, 1, plane, at.y] + one[j, 1, k]
            b = go(send(total.at[j, 1, k, 1 - at.x], two.at[j, 1, k], s_two.at[j, k, 1], r_two.at[j, k, 1], "fs", at.fx))
            second_stage[k] = (a, b)
            if k + 3 < depth:
                stage_one(k + 3)

        def stage_three(k):
            third_stage[k] = []
            for h, keep in enumerate((at.y, at.x)):
                second_stage[k][h].wait_recv()
                ready[j, h, k] = total[j, h, k, keep] + two[j, h, k]
                if k < depth - 1:
                    target = at.column(depth - 1 - k)
                    third_stage[k].append(
                        go(send(ready.at[j, h, k], far.at[j, h, k], s_far.at[j, k, h], r_far.at[j, k, h], "fs", target))
                    )

        def prefetch():
            for k in range(min(3, depth)):
                stage_one(k)
            after_first()

        events = [(start, prefetch)]
        last = start
        for k in range(depth):
            when = start + HOP + unit * (k + 1) + 0.5 * unit * max(0, k - 1)
            events.append((when, functools.partial(stage_two, k)))
            last = when + HOP + unit
            events.append((last, functools.partial(stage_three, k)))
        yield from in_order(events)
        yield last + HOP + unit
        for h in range(2):
            low = ready[j, h, depth - 1]
            for k in range(depth - 1):
                third_stage[k][h].wait_recv()
                low = low + far[j, h, k]
            side = slice(h * half, (h + 1) * half)
            new_first, new_second, ratio = moments(low, first[i, :, side], second[i, :, side])
            first_out[i, :, side] = new_first
            second_out[i, :, side] = new_second
            ratios[j, h, at.f] = ratio

    def direct(j, i):
        square = None
        for h in range(2):
            wide = ratios[j, h].reshape(rank, half)
            direction = None
            grown = None
            for k, part in enumerate(split(wide)):
                product = dot(left[i, 0 : rows + (3 - k) * rank], part)
                piece = product[0:rows]
                direction = piece if direction is None else direction + piece
                for g in range(3 - k):
                    piece = product[rows + g * rank : rows + (g + 1) * rank]
                    grown = piece if grown is None else grown + piece
            step[i, :, h * half : (h + 1) * half] = direction
            value = jnp.sum(wide * grown)
            square = value if square is None else square + value
        pair[j, 0] = jnp.full((8, 128), square, jnp.float32)
        return [
            go(send(pair.at[j, 0], pair.at[j, k + 1], s_tp.at[j, k], r_tp.at[j, k], "tp", o)) for k, o in enumerate(mates)
        ]

    def finish(j, i, trips):
        joint = pair[j, 0]
        for k, trip in enumerate(trips):
            trip.wait_recv()
            joint = joint + pair[j, k + 1]
        count = n * rows * m * cols
        scale = lax.rsqrt(jnp.maximum(joint, 0.0) / count + mean_floor)
        new_step = step[i] * scale[0:1, 0:1]
        step[i] = new_step
        copies[i, at.f] = (master[i] - step_size * new_step).astype(jnp.bfloat16)

    def sems_of(group, j):
        return [s.at[j] for s in group]

    def stream(j, i, plan):
        begin, scatter, ratio_time, direct_time, copy_time = plan
        yield begin
        cot_loads[j].wait()

        @pl.when(own != j)
        def _():
            mid_trip.wait_recv()

        project(j, i)

        def after_first():
            if j == 0:
                find_gram(own)
                gram_trip.append(
                    go(send(left.at[own, gram], left.at[own, gram], s_mate.at[1], r_mate.at[1], "tp", mate))
                )
                for copy in other_loads:
                    copy.wait()

        yield from reduce_scatter(j, i, scatter, after_first)
        yield from gather(
            at,
            go,
            lambda h, index: ratios.at[j, h, index],
            sems_of(ratio_sems, j),
            ratio_time,
            low_rows * half * 4 / RATE,
        )
        yield direct_time

        @pl.when(own != j)
        def _():
            gram_trip[0].wait_recv()

        trips = direct(j, i)
        yield direct_time + 1.5
        finish(j, i, trips)
        size = rows // 2
        yield from gather(
            at,
            go,
            lambda h, index: copies.at[i, index, pl.ds(h * size, size)],
            sems_of(copy_sems, j),
            copy_time,
            size * cols * 2 / RATE,
        )

    body = n * rows * cols * 2 * 5 / 16 / RATE
    merge(
        [
            stream(0, 0, (0.0, 1.0, 15.0, 28.0, 31.0)),
            stream(1, 1, (2.5, 8.0, 22.5, 38.0, 29.0 + body)),
        ]
    )
    for copy in started:
        copy.wait_send()


def hand_kernel(depth, *refs):
    step, first, second, copies = refs[:4]
    outs = refs[4:12]
    sem = refs[12]
    moves = []
    for k, (src, dst) in enumerate(
        (
            (step.at[0], outs[0]),
            (step.at[1], outs[1]),
            (first.at[0], outs[2]),
            (second.at[0], outs[3]),
            (first.at[1], outs[4]),
            (second.at[1], outs[5]),
            (copies.at[0], outs[6]),
            (copies.at[1], outs[7]),
        )
    ):
        pieces = depth if len(dst.shape) == 3 else 1
        size = dst.shape[0] // pieces
        for p in range(pieces):
            part = pl.ds(p * size, size)
            moves.append(pltpu.make_async_copy(src.at[part], dst.at[part], sem.at[k, p]))
    for move in moves:
        move.start()
    for move in moves:
        move.wait()


def local(
    n,
    m,
    saved_inputs,
    input_cot,
    gate_cot,
    input_master,
    gate_master,
    input_factor,
    gate_factor,
    input_first,
    input_second,
    gate_first,
    gate_second,
):
    anywhere = pl.BlockSpec(memory_space=pl.ANY)
    in_vmem = pl.BlockSpec(memory_space=VMEM)
    rows, rank = input_factor.shape
    tokens = saved_inputs.shape[0]
    low_rows, cols = input_first.shape
    depth = n // PLANE
    half = cols // 2
    shape = jax.ShapeDtypeStruct
    f32, bf16 = jnp.float32, jnp.bfloat16
    held = [
        VMEM((2, rows, cols), f32),
        VMEM((2, low_rows, cols), f32),
        VMEM((2, low_rows, cols), f32),
        VMEM((2, n, rows, cols), bf16),
    ]
    outs = pl.pallas_call(
        functools.partial(main_kernel, n, m),
        out_shape=held,
        in_specs=[anywhere] * 11,
        out_specs=[in_vmem] * 4,
        scratch_shapes=[
            VMEM(saved_inputs.shape, bf16),
            VMEM((2,) + input_cot.shape, bf16),
            VMEM((2, rows, cols), f32),
            VMEM((2, rows + 3 * rank, rank), bf16),
            VMEM((2, low_rows, cols), f32),
            VMEM((2, low_rows, cols), f32),
            VMEM((n, rows, rank), bf16),
            VMEM((2, tokens, rank), f32),
            VMEM((2, 2, depth, 2, 2, low_rows, half), f32),
            VMEM((2, 2, depth, 2, low_rows, half), f32),
            VMEM((2, 2, depth, 2, low_rows, half), f32),
            VMEM((2, 2, depth, low_rows, half), f32),
            VMEM((2, 2, depth, low_rows, half), f32),
            VMEM((2, 2, depth, low_rows, half), f32),
            VMEM((2, 2, n, low_rows, half), f32),
            VMEM((2, m, 8, 128), f32),
            DMA((11,)),
            DMA((2,)),
            DMA((2,)),
            *[DMA((2, depth, 2))] * 6,
            DMA((2, m)),
            DMA((2, m)),
            *gather_sems(n),
            *gather_sems(n, 2),
            *gather_sems(n, 2),
        ],
        compiler_params=pltpu.CompilerParams(collective_id=1, has_side_effects=True, vmem_limit_bytes=50 * 2**20),
        name="update",
    )(
        saved_inputs,
        input_cot,
        gate_cot,
        input_master,
        gate_master,
        input_factor,
        gate_factor,
        input_first,
        input_second,
        gate_first,
        gate_second,
    )
    outs = [pltpu.with_memory_space_constraint(x, VMEM) for x in outs]
    full = shape((rows, cols), f32)
    low = shape((low_rows, cols), f32)
    block = shape((n, rows, cols), bf16)
    outs = pl.pallas_call(
        functools.partial(hand_kernel, depth),
        out_shape=[full, full, low, low, low, low, block, block],
        in_specs=[in_vmem] * 4,
        out_specs=[anywhere] * 8,
        scratch_shapes=[DMA((8, depth))],
        compiler_params=pltpu.CompilerParams(vmem_limit_bytes=2**20),
        name="results",
    )(*outs)
    *head, copy_in, copy_gate = outs
    return (*head, copy_in.reshape(n * rows, cols), copy_gate.reshape(n * rows, cols))


def solution(mesh):
    n, m = mesh.shape["fs"], mesh.shape["tp"]
    both = P("fs", "tp")
    rows = P("fs", None)
    return jax.shard_map(
        functools.partial(local, n, m),
        mesh=mesh,
        in_specs=(rows, both, both, both, both, rows, rows, both, both, both, both),
        out_specs=(both,) * 6 + (P(None, "tp"),) * 2,
        check_vma=False,
    )
```

time: 167 us -> 150 us (0.90)
  Pallas kernels: 166 us -> 149 us
    pallas_call x2, Pallas kernels: 166 us -> 149 us  [the longest x1 145 us: local(): pl.pallas_call(functools.partial(main_kernel, n, m), out_shape=held, in_s...]
where the time goes in v1:
time: 150 us
  Pallas kernels  149 us (99%)
    pallas_call x1, Pallas kernels, local(): pl.pallas_call(functools.partial(main_kernel, n, m), out_shape=held, in_s...  145 us
    pallas_call x1, Pallas kernels, local(): pl.pallas_call(functools.partial(hand_kernel, depth), out_shape=[full, fu...  3.98 us

profile of v1, /device:TPU:0, one launch (start us, length us, event | category | flops | bytes accessed | tf_op | source)
XLA Modules:
  0.0 150.1 jit_solution(17396174252985868155)
XLA Ops:
  0.6 145.4 %update.1 = (f32[2,128,1024]{2,1,0:T(8,128)S(1)}, f32[2,16,1024]{2,1,0:T(8,128)S(1)}, f32[2,16,1024]{2,1,0:T(8,128)S(1)}, bf16[2,16,128,1024]{3,2,1,0:T(8,128)(2,1)S(1)}) custom-call(bf16[768,2048]{1,0:T(8,128)(2,1)} %refs_0_.1, bf16[768,1024]{1,0:T(8,128)(2,1)} %refs_1_.1, bf16[768,1024]{1,0:T(8,128)(2,1)} %refs_2_.1, f32[128,1024]{1,0:T(8,128)} %refs_3_.1, ...), custom_call_target="tpu_custom_call" | custom-call | tf_op jit(solution)/shard_map/update/pallas_call | solution.py:508
  146.1 4.0 %results.1 = (f32[128,1024]{1,0:T(8,128)}, f32[128,1024]{1,0:T(8,128)}, f32[16,1024]{1,0:T(8,128)}, f32[16,1024]{1,0:T(8,128)}, f32[16,1024]{1,0:T(8,128)}, /*in...) custom-call(f32[2,128,1024]{2,1,0:T(8,128)S(1)} %get-tuple-element.20.refs_0_, ...), custom_call_target="tpu_custom_call" | custom-call | tf_op jit(solution)/shard_map/results/pallas_call | solution.py:559

commit v2 on v1

--- a/solution.py
+++ b/solution.py
@@ -96,9 +96,8 @@
             waited.add(id(copy))
             copy.wait_recv()
 
-    def reach():
-        for s in range(1, depth):
-            far[s] = [hop(h, at.f, s_z.at[s, h], r_z.at[s, h], at.column(s)) for h in range(2)]
+    def reach(s):
+        far[s] = [hop(h, at.f, s_z.at[s, h], r_z.at[s, h], at.column(s)) for h in range(2)]
 
     def issue(s):
         mine = at.column(s)
@@ -112,7 +111,6 @@
 
         if s == 0:
             x(0, 0), y(1, 2), y(0, 1), x(1, 3)
-            reach()
         else:
             need(far[s][0])
             x(0, 0), y(0, 1)
@@ -144,6 +142,8 @@
     for s in range(depth):
         when = free if s == 0 else max(free, start + 2 * unit * s + HOP)
         events.append((when, functools.partial(issue, s)))
+        if s + 1 < depth:
+            events.append((start + 1.9 * unit * s, functools.partial(reach, s + 1)))
         if s % 2 == 0:
             free = when + 3 * unit
             cornered = when + 3 * unit + 2 * HOP
@@ -167,6 +167,125 @@
     yield from in_order(fixed)
 
 
+def line_gather(at, go, go_if, view, sems, start, unit):
+    s_z, r_z, s_p, r_p = sems
+    inner = lax.rem(at.z + 1, at.depth) >= at.depth // 2
+    outer = jnp.logical_not(inner)
+    mixed = inner.astype(jnp.int32)
+    one, two, three = at.twin(1), at.twin(2), at.twin(3)
+    planes = [at.z, one, two + mixed * (three - two), three + mixed * (two - three)]
+    bases = [plane * PLANE for plane in planes]
+    partner = one * PLANE + at.spot
+    across = three * PLANE + at.spot
+    near = {}
+    waited = set()
+
+    def along(half, index, slot, place, target, when=None):
+        ref = view(half, index)
+        copy = send(ref, ref, s_z.at[slot, half], r_z.at[place, half], "fs", target)
+        go(copy) if when is None else go_if(when, copy)
+
+    def landed(half, index, place):
+        ref = view(half, index)
+        send(ref, ref, s_z.at[0, half], r_z.at[place, half], "fs", partner).wait_recv()
+
+    def need(copy):
+        if id(copy) not in waited:
+            waited.add(id(copy))
+            copy.wait_recv()
+
+    def issue(q):
+        mine = bases[q] + at.spot
+        got = near[q] = {}
+
+        def hop(half, k, target):
+            ref = view(half, mine)
+            got[k] = go(send(ref, ref, s_p.at[q, k], r_p.at[q, k], "fs", target))
+
+        if q:
+
+            @pl.when(outer)
+            def _():
+                for half in range(2):
+                    landed(half, mine, q)
+
+        hop(0, 0, at.fx), hop(1, 2, at.fy), hop(0, 1, at.fy), hop(1, 3, at.fx)
+        if q == 0:
+            for half in range(2):
+                along(half, mine, 0, 1, partner)
+                along(half, mine, 1, 2, across, inner)
+
+    def forward(q, half):
+        index = bases[q] + at.spot
+
+        @pl.when(inner)
+        def _():
+            landed(half, index, q)
+
+        along(half, index, 1 + q, 3 if q == 1 else q, across if q == 1 else partner, inner)
+
+    def relay(q):
+        for half, k, other, target in ((0, 0, at.sx, at.fy), (1, 2, at.sy, at.fx)):
+            need(near[q][k])
+            ref = view(half, bases[q] + other)
+            near[q][4 + half] = go(send(ref, ref, s_p.at[q, 4 + half], r_p.at[q, 4 + half], "fs", target))
+
+    def corner(half):
+        index = bases[0] + PLANE - 1 - at.spot
+        need(near[0][4 + half])
+        along(half, index, 5, 4, partner)
+        along(half, index, 6, 5, across, inner)
+
+    def pass_corner(half):
+        index = bases[2] + PLANE - 1 - at.spot
+
+        @pl.when(inner)
+        def _():
+            landed(half, index, 5)
+
+        along(half, index, 7, 5, partner, inner)
+
+    def done():
+        for q in range(4):
+            for k in sorted(near[q]):
+                need(near[q][k])
+        for half in range(2):
+            landed(half, bases[1] + PLANE - 1 - at.spot, 4)
+
+            @pl.when(outer)
+            def _():
+                landed(half, bases[2] + PLANE - 1 - at.spot, 5)
+
+    def at_time(when, act, *args):
+        return (start + when, functools.partial(act, *args))
+
+    first, second = unit + HOP, 2 * unit + HOP
+    events = [
+        at_time(0.0, issue, 0),
+        at_time(first, forward, 1, 0),
+        at_time(first + 0.01, forward, 2, 0),
+        at_time(first + 0.02, relay, 0),
+        at_time(second, forward, 1, 1),
+        at_time(second + 0.01, forward, 2, 1),
+        at_time(second + 0.02, issue, 1),
+        at_time(first + 2 * unit, forward, 3, 0),
+        at_time(second + 2 * unit, forward, 3, 1),
+        at_time(second + 2 * unit + 0.005, corner, 0),
+        at_time(second + 2 * unit + 0.006, corner, 1),
+        at_time(second + 2 * unit + 0.01, issue, 2),
+        at_time(4 * unit + 3 * HOP, pass_corner, 0),
+        at_time(second + 4 * unit, issue, 3),
+        at_time(5 * unit + 3 * HOP, pass_corner, 1),
+        at_time(8 * unit + HOP, relay, 3),
+        at_time(10 * unit + 2 * HOP, done),
+    ]
+    yield from in_order(events)
+
+
+def line_sems(copies):
+    return [DMA((copies, 8, 2)), DMA((copies, 6, 2)), DMA((copies, 4, 6)), DMA((copies, 4, 6))]
+
+
 def gather_sems(n, copies=None):
     depth = n // PLANE
     lead = () if copies is None else (copies,)
@@ -246,6 +365,15 @@
         started.append(copy)
         return copy
 
+    asked = []
+
+    def go_if(when, copy):
+        @pl.when(when)
+        def _():
+            copy.start()
+
+        asked.append((when, copy))
+
     for copy in factor_loads:
         copy.wait()
 
@@ -427,14 +555,12 @@
         yield direct_time + 1.5
         finish(j, i, trips)
         size = rows // 2
-        yield from gather(
-            at,
-            go,
-            lambda h, index: copies.at[i, index, pl.ds(h * size, size)],
-            sems_of(copy_sems, j),
-            copy_time,
-            size * cols * 2 / RATE,
-        )
+        view = lambda h, index: copies.at[i, index, pl.ds(h * size, size)]
+        unit = size * cols * 2 / RATE
+        if depth == 4:
+            yield from line_gather(at, go, go_if, view, sems_of(copy_sems, j), copy_time, unit)
+        else:
+            yield from gather(at, go, view, sems_of(copy_sems, j), copy_time, unit)
 
     body = n * rows * cols * 2 * 5 / 16 / RATE
     merge(
@@ -445,6 +571,11 @@
     )
     for copy in started:
         copy.wait_send()
+    for when, copy in asked:
+
+        @pl.when(when)
+        def _():
+            copy.wait_send()
 
 
 def hand_kernel(depth, *refs):
@@ -535,7 +666,7 @@
             DMA((2, m)),
             *gather_sems(n),
             *gather_sems(n, 2),
-            *gather_sems(n, 2),
+            *(line_sems(2) if depth == 4 else gather_sems(n, 2)),
         ],
         compiler_params=pltpu.CompilerParams(collective_id=1, has_side_effects=True, vmem_limit_bytes=50 * 2**20),
         name="update",

time: 150 us -> 135 us (0.900)
  Pallas kernels: 149 us -> 134 us
    pallas_call x1, Pallas kernels: 145 us -> 130 us  [local(): pl.pallas_call(functools.partial(main_kernel, n, m), out_shape=held, in_s...]
where the time goes in v2:
time: 135 us
  Pallas kernels  134 us (99%)
    pallas_call x1, Pallas kernels, local(): pl.pallas_call(functools.partial(main_kernel, n, m), out_shape=held, in_s...  130 us
    pallas_call x1, Pallas kernels, local(): pl.pallas_call(functools.partial(hand_kernel, depth), out_shape=[full, fu...  3.98 us

profile of v2, /device:TPU:0, one launch (start us, length us, event | category | flops | bytes accessed | tf_op | source)
XLA Modules:
  0.0 134.6 jit_solution(5526910302728606829)
XLA Ops:
  0.6 129.9 %update.1 = (f32[2,128,1024]{2,1,0:T(8,128)S(1)}, f32[2,16,1024]{2,1,0:T(8,128)S(1)}, f32[2,16,1024]{2,1,0:T(8,128)S(1)}, bf16[2,16,128,1024]{3,2,1,0:T(8,128)(2,1)S(1)}) custom-call(bf16[768,2048]{1,0:T(8,128)(2,1)} %refs_0_.1, bf16[768,1024]{1,0:T(8,128)(2,1)} %refs_1_.1, bf16[768,1024]{1,0:T(8,128)(2,1)} %refs_2_.1, f32[128,1024]{1,0:T(8,128)} %refs_3_.1, ...), custom_call_target="tpu_custom_call" | custom-call | tf_op jit(solution)/shard_map/update/pallas_call | solution.py:639
  130.6 4.0 %results.1 = (f32[128,1024]{1,0:T(8,128)}, f32[128,1024]{1,0:T(8,128)}, f32[16,1024]{1,0:T(8,128)}, f32[16,1024]{1,0:T(8,128)}, f32[16,1024]{1,0:T(8,128)}, /*in...) custom-call(f32[2,128,1024]{2,1,0:T(8,128)S(1)} %get-tuple-element.20.refs_0_, ...), custom_call_target="tpu_custom_call" | custom-call | tf_op jit(solution)/shard_map/results/pallas_call | solution.py:690

commit v3 on v2

--- a/solution.py
+++ b/solution.py
@@ -13,7 +13,7 @@
 mean_floor = 1e-06
 step_size = 0.05
 PLANE = 4
-HOP = 2.0
+HOP = 2.8
 RATE = 46600.0
 VMEM = pltpu.VMEM
 DMA = pltpu.SemaphoreType.DMA
@@ -31,6 +31,7 @@
         self.y = lax.div(self.spot, 2)
         self.fx = self.f + 1 - 2 * self.x
         self.fy = self.f + 2 - 4 * self.y
+        self.fd = self.fx + 2 - 4 * self.y
         self.sx = self.spot + 1 - 2 * self.x
         self.sy = self.spot + 2 - 4 * self.y
 
@@ -65,6 +66,32 @@
     pl.semaphore_wait(barrier, len(targets))
 
 
+class Bank:
+    def __init__(self, ref, lead, base, *sizes):
+        self.ref, self.lead, self.base, self.sizes = ref, lead, base, sizes
+        self.at = self
+
+    def __getitem__(self, index):
+        flat = 0
+        for i, size in zip(index if isinstance(index, tuple) else (index,), self.sizes):
+            flat = flat * size + i
+        return self.ref.at[self.lead, self.base + flat]
+
+
+def banks(sends, recvs, lead, base, *shapes):
+    made = []
+    for send_shape, recv_shape in shapes:
+        made += [Bank(sends, lead, base[0], *send_shape), Bank(recvs, lead, base[1], *recv_shape)]
+        base = (base[0] + functools.reduce(int.__mul__, send_shape), base[1] + functools.reduce(int.__mul__, recv_shape))
+    return made
+
+
+def gather_shapes(depth):
+    if depth == 4:
+        return (((7, 2), (6, 2)), ((4, 6), (4, 6)))
+    return (((depth, 2), (depth, 2)), ((depth, 6), (depth, 6)))
+
+
 def merge(streams):
     heads = [[next(g, None), g] for g in streams]
     while True:
@@ -81,7 +108,7 @@
         act()
 
 
-def gather(at, go, view, sems, start, unit, arrived=None):
+def gather(at, go, view, sems, start, unit, also):
     s_z, r_z, s_p, r_p = sems
     depth = at.depth
     far, near = {}, {}
@@ -133,8 +160,6 @@
     def done(s):
         for k in sorted(near[s]):
             need(near[s][k])
-        if arrived is not None:
-            arrived(at.twin(s) * PLANE)
 
     events = []
     free = start
@@ -164,10 +189,11 @@
         if act.func is corner:
             when = max(when, times[act.args[0] + 1] + 0.01)
         fixed.append((when, act))
+    fixed += [(start + when * unit, act) for when, act in also]
     yield from in_order(fixed)
 
 
-def line_gather(at, go, go_if, view, sems, start, unit):
+def line_gather(at, go, go_if, view, sems, start, unit, also):
     s_z, r_z, s_p, r_p = sems
     inner = lax.rem(at.z + 1, at.depth) >= at.depth // 2
     outer = jnp.logical_not(inner)
@@ -177,6 +203,8 @@
     bases = [plane * PLANE for plane in planes]
     partner = one * PLANE + at.spot
     across = three * PLANE + at.spot
+    second_target = (two + mixed * (three - two)) * PLANE + at.spot
+    second_place = 3 - mixed
     near = {}
     waited = set()
 
@@ -202,7 +230,10 @@
             ref = view(half, mine)
             got[k] = go(send(ref, ref, s_p.at[q, k], r_p.at[q, k], "fs", target))
 
-        if q:
+        if q == 1:
+            for half in range(2):
+                landed(half, mine, q)
+        elif q:
 
             @pl.when(outer)
             def _():
@@ -213,7 +244,7 @@
         if q == 0:
             for half in range(2):
                 along(half, mine, 0, 1, partner)
-                along(half, mine, 1, 2, across, inner)
+                along(half, mine, 1, second_place, second_target)
 
     def forward(q, half):
         index = bases[q] + at.spot
@@ -222,7 +253,7 @@
         def _():
             landed(half, index, q)
 
-        along(half, index, 1 + q, 3 if q == 1 else q, across if q == 1 else partner, inner)
+        along(half, index, q, q, partner, inner)
 
     def relay(q):
         for half, k, other, target in ((0, 0, at.sx, at.fy), (1, 2, at.sy, at.fx)):
@@ -233,8 +264,8 @@
     def corner(half):
         index = bases[0] + PLANE - 1 - at.spot
         need(near[0][4 + half])
-        along(half, index, 5, 4, partner)
-        along(half, index, 6, 5, across, inner)
+        along(half, index, 4, 4, partner)
+        along(half, index, 5, 5, across, inner)
 
     def pass_corner(half):
         index = bases[2] + PLANE - 1 - at.spot
@@ -243,7 +274,7 @@
         def _():
             landed(half, index, 5)
 
-        along(half, index, 7, 5, partner, inner)
+        along(half, index, 6, 5, partner, inner)
 
     def done():
         for q in range(4):
@@ -260,36 +291,26 @@
         return (start + when, functools.partial(act, *args))
 
     first, second = unit + HOP, 2 * unit + HOP
+    third = max(5 * unit + 2 * HOP + 1.0, 7 * unit)
     events = [
         at_time(0.0, issue, 0),
-        at_time(first, forward, 1, 0),
-        at_time(first + 0.01, forward, 2, 0),
+        at_time(first, forward, 2, 0),
         at_time(first + 0.02, relay, 0),
-        at_time(second, forward, 1, 1),
-        at_time(second + 0.01, forward, 2, 1),
-        at_time(second + 0.02, issue, 1),
-        at_time(first + 2 * unit, forward, 3, 0),
-        at_time(second + 2 * unit, forward, 3, 1),
-        at_time(second + 2 * unit + 0.005, corner, 0),
-        at_time(second + 2 * unit + 0.006, corner, 1),
-        at_time(second + 2 * unit + 0.01, issue, 2),
+        at_time(second, forward, 2, 1),
+        at_time(second + 0.01, issue, 1),
+        at_time(first + 2 * unit + 1.0, forward, 3, 0),
+        at_time(first + 3 * unit + 1.0, forward, 3, 1),
+        at_time(first + 3 * unit + 1.0 + HOP, corner, 0),
+        at_time(first + 3 * unit + 1.01 + HOP, corner, 1),
+        at_time(max(first + 3 * unit + 1.02, 3 * unit + 2 * HOP), issue, 2),
         at_time(4 * unit + 3 * HOP, pass_corner, 0),
-        at_time(second + 4 * unit, issue, 3),
         at_time(5 * unit + 3 * HOP, pass_corner, 1),
-        at_time(8 * unit + HOP, relay, 3),
-        at_time(10 * unit + 2 * HOP, done),
+        at_time(third, issue, 3),
+        at_time(third + unit + HOP, relay, 3),
+        at_time(max(third + 4 * unit + 2 * HOP, 6 * unit + 4 * HOP), done),
     ]
+    events += [(start + when * unit, act) for when, act in also]
     yield from in_order(events)
-
-
-def line_sems(copies):
-    return [DMA((copies, 8, 2)), DMA((copies, 6, 2)), DMA((copies, 4, 6)), DMA((copies, 4, 6))]
-
-
-def gather_sems(n, copies=None):
-    depth = n // PLANE
-    lead = () if copies is None else (copies,)
-    return [DMA(lead + (depth, 2)), DMA(lead + (depth, 2)), DMA(lead + (depth, 6)), DMA(lead + (depth, 6))]
 
 
 def moments(low_rank, first, second):
@@ -319,14 +340,13 @@
         step, first_out, second_out, copies,
         saved, cot, master, left, first, second, whole, mid, term,
         one, total, two, ready, far, ratios, pair,
-        load_sem, s_mate, r_mate, s_one, r_one, s_two, r_two, s_far, r_far, s_tp, r_tp,
-        *rest,
+        load_sem, s_mate, r_mate, s_gram, r_gram, s_tp, r_tp, s_pool, r_pool, s_ratio, r_ratio,
     ) = refs
-    factor_sems, ratio_sems, copy_sems = rest[0:4], rest[4:8], rest[8:12]
     at = Place(n)
     depth = at.depth
     t = lax.axis_index("tp")
-    own = lax.rem(t, 2) if m % 2 == 0 else 0
+    parts = 2 if m % 2 == 0 else 1
+    own = lax.rem(t, 2) if parts == 2 else 0
     mate = t + 1 - 2 * own
     mates = [lax.rem(t + k, m) for k in range(1, m)]
     rows, rank = factor_a_hbm.shape
@@ -357,7 +377,7 @@
             )
         )
     ]
-    greet([("fs", at.fx), ("fs", at.fy)] + [("fs", at.column(s)) for s in range(1, depth)] + [("tp", o) for o in mates])
+    greet([("fs", at.fx), ("fs", at.fy), ("fs", at.fd)] + [("fs", at.column(s)) for s in range(1, depth)] + [("tp", o) for o in mates])
     started = []
 
     def go(copy):
@@ -377,73 +397,100 @@
     for copy in factor_loads:
         copy.wait()
 
-    def factor_gather(j, i, start):
-        multiplied = []
-        whole[at.f] = left[i, 0:rows]
-
-        def arrived(base):
-            if not multiplied:
-                if j == 0:
-                    saved_load.wait()
+    size = rows // parts
+    mine = pl.ds(pl.multiple_of(own * size, size), size)
+
+    def factor_gather(j, start, swap_start, multiply_start, pace):
+        s_z, r_z, s_p, r_p = banks(s_pool, r_pool, j, (0, 0), ((depth,), (depth,)), ((depth, 3), (depth, 3)))
+        unit = size * rank * 2 / RATE
+        whole[j, at.f, mine] = left[j, mine]
+        far, near, swaps = {}, {}, {}
+
+        def hop(index, s_sem, r_sem, target):
+            ref = whole.at[j, index, mine]
+            return go(send(ref, ref, s_sem, r_sem, "fs", target))
+
+        def begin():
+            for s in range(depth - 1, 0, -1):
+                far[s] = hop(at.f, s_z.at[s], r_z.at[s], at.column(s))
+            issue(0)
+
+        def issue(s):
+            if s:
+                far[s].wait_recv()
+            near[s] = [hop(at.column(s), s_p.at[s, k], r_p.at[s, k], o) for k, o in enumerate((at.fd, at.fx, at.fy))]
+
+        def swap(s):
+            for copy in near[s]:
+                copy.wait_recv()
+            if parts == 2:
+                view = whole.at[j, pl.ds(at.twin(s) * PLANE, PLANE), mine]
+                swaps[s] = go(send(view, view, s_mate.at[j, s], r_mate.at[j, s], "tp", mate))
+
+        def multiply(s):
+            if parts == 2:
+                swaps[s].wait_recv()
+            if s == 0 and j == 0:
+                saved_load.wait()
+            base = at.twin(s) * PLANE
             columns = pl.ds(pl.multiple_of(base * rows, width), width)
-            product = dot(saved[:, columns], whole[pl.ds(base, PLANE)].reshape(width, rank))
-            if multiplied:
-                mid[i] += product
+            product = dot(saved[:, columns], whole[j, pl.ds(base, PLANE)].reshape(width, rank))
+            if s == 0:
+                mid[j] = product
             else:
-                mid[i] = product
-            multiplied.append(base)
-
-        size = rows // 2
-        yield from gather(
-            at,
-            go,
-            lambda h, index: whole.at[index, pl.ds(h * size, size)],
-            factor_sems,
-            start,
-            size * rank * 2 / RATE,
-            arrived,
-        )
+                mid[j] += product
+
+        events = [(start, begin)]
+        for s in range(depth):
+            when = start + 0.01 if s == 0 else start + 2.0 + 0.7 * s
+            if s:
+                events.append((when, functools.partial(issue, s)))
+            swap_at = max(swap_start + pace * s, when + 0.01)
+            multiply_at = max(multiply_start + (pace if j == 0 else 0.3) * s, swap_at + 0.01)
+            events.append((swap_at, functools.partial(swap, s)))
+            events.append((multiply_at, functools.partial(multiply, s)))
+        yield from in_order(events)
 
     def find_gram(i):
-        factor = whole[...].reshape(n * rows, rank)
+        factor = whole[i].reshape(n * rows, rank)
         product = lax.dot_general(factor, factor, (((0,), (0,)), ((), ())), preferred_element_type=jnp.float32)
         for k, part in enumerate(split(product)):
             left[i, rows + k * rank : rows + (k + 1) * rank] = part
 
-    merge([factor_gather(0, own, 0.0)])
-    mid_trip = go(send(mid.at[own], mid.at[own], s_mate.at[0], r_mate.at[0], "tp", mate))
     gram_trip = []
 
-    def project(j, i):
-        result = None
-        for part in split(mid[i].T):
-            piece = dot(part, cot[i])
-            result = piece if result is None else result + piece
-        for h in range(2):
-            term[j, h] = result[:, h * half : (h + 1) * half].reshape(depth, 2, 2, low_rows, half)
-
-    def reduce_scatter(j, i, start, after_first):
+    def project(j, h):
+        parts_of = jnp.concatenate(split(mid[j].T), axis=0)
+        product = dot(parts_of, cot[j, :, h * half : (h + 1) * half])
+        result = product[0:rank] + product[rank : 2 * rank] + product[2 * rank : 3 * rank]
+        term[j, h] = result.reshape(depth, 2, 2, low_rows, half)
+
+    def reduce_scatter(j, i, project_at, gap, start, pace, ahead, hold):
         unit = 2 * low_rows * half * 4 / RATE
+        stages = [((depth, 2), (depth, 2))] * 3
+        s_one, r_one, s_two, r_two, s_far, r_far = banks(s_pool, r_pool, j, (4 * depth, 4 * depth), *stages)
         first_stage, second_stage, third_stage = {}, {}, {}
 
-        def stage_one(k):
+        def stage_one(k, halves=(0, 1)):
             plane = at.twin(depth - 1 - k)
-            first_stage[k] = (
-                go(send(term.at[j, 0, plane, :, 1 - at.x], one.at[j, 0, k], s_one.at[j, k, 0], r_one.at[j, k, 0], "fs", at.fx)),
-                go(send(term.at[j, 1, plane, 1 - at.y], one.at[j, 1, k], s_one.at[j, k, 1], r_one.at[j, k, 1], "fs", at.fy)),
-            )
+            for h in halves:
+                src, target = (
+                    (term.at[j, 0, plane, :, 1 - at.x], at.fx) if h == 0 else (term.at[j, 1, plane, 1 - at.y], at.fy)
+                )
+                copy = go(send(src, one.at[j, h, k], s_one.at[k, h], r_one.at[k, h], "fs", target))
+                first_stage.setdefault(k, []).append(copy)
 
         def stage_two(k):
             plane = at.twin(depth - 1 - k)
             first_stage[k][0].wait_recv()
             total[j, 0, k] = term[j, 0, plane, :, at.x] + one[j, 0, k]
-            a = go(send(total.at[j, 0, k, 1 - at.y], two.at[j, 0, k], s_two.at[j, k, 0], r_two.at[j, k, 0], "fs", at.fy))
+            a = go(send(total.at[j, 0, k, 1 - at.y], two.at[j, 0, k], s_two.at[k, 0], r_two.at[k, 0], "fs", at.fy))
             first_stage[k][1].wait_recv()
             total[j, 1, k] = term[j, 1, plane, at.y] + one[j, 1, k]
-            b = go(send(total.at[j, 1, k, 1 - at.x], two.at[j, 1, k], s_two.at[j, k, 1], r_two.at[j, k, 1], "fs", at.fx))
+            b = go(send(total.at[j, 1, k, 1 - at.x], two.at[j, 1, k], s_two.at[k, 1], r_two.at[k, 1], "fs", at.fx))
             second_stage[k] = (a, b)
-            if k + 3 < depth:
-                stage_one(k + 3)
+            if ahead and k + ahead < depth:
+                stage_one(k + ahead)
 
         def stage_three(k):
             third_stage[k] = []
@@ -453,20 +500,25 @@
                 if k < depth - 1:
                     target = at.column(depth - 1 - k)
                     third_stage[k].append(
-                        go(send(ready.at[j, h, k], far.at[j, h, k], s_far.at[j, k, h], r_far.at[j, k, h], "fs", target))
+                        go(send(ready.at[j, h, k], far.at[j, h, k], s_far.at[k, h], r_far.at[k, h], "fs", target))
                     )
 
-        def prefetch():
-            for k in range(min(3, depth)):
-                stage_one(k)
-            after_first()
-
-        events = [(start, prefetch)]
+        def prefetch(h):
+            project(j, h)
+            for k in range(min(ahead, depth)):
+                stage_one(k, (h,))
+            if h and j == 0:
+                for copy in other_loads:
+                    copy.wait()
+
+        events = [(project_at + gap * h, functools.partial(prefetch, h)) for h in range(2)]
+        if ahead == 0:
+            events += [(start + pace * k, functools.partial(stage_one, k)) for k in range(depth)]
         last = start
         for k in range(depth):
-            when = start + HOP + unit * (k + 1) + 0.5 * unit * max(0, k - 1)
+            when = start + HOP + unit + pace * k
             events.append((when, functools.partial(stage_two, k)))
-            last = when + HOP + unit
+            last = max(when + HOP + 0.5 * unit, hold + 0.01 * k)
             events.append((last, functools.partial(stage_three, k)))
         yield from in_order(events)
         yield last + HOP + unit
@@ -483,24 +535,29 @@
 
     def direct(j, i):
         square = None
+        pieces = []
         for h in range(2):
             wide = ratios[j, h].reshape(rank, half)
-            direction = None
             grown = None
-            for k, part in enumerate(split(wide)):
-                product = dot(left[i, 0 : rows + (3 - k) * rank], part)
-                piece = product[0:rows]
-                direction = piece if direction is None else direction + piece
+            pieces.append(split(wide))
+            for k, part in enumerate(pieces[h]):
+                product = dot(left[i, rows : rows + (3 - k) * rank], part)
                 for g in range(3 - k):
-                    piece = product[rows + g * rank : rows + (g + 1) * rank]
+                    piece = product[g * rank : (g + 1) * rank]
                     grown = piece if grown is None else grown + piece
-            step[i, :, h * half : (h + 1) * half] = direction
             value = jnp.sum(wide * grown)
             square = value if square is None else square + value
         pair[j, 0] = jnp.full((8, 128), square, jnp.float32)
-        return [
+        trips = [
             go(send(pair.at[j, 0], pair.at[j, k + 1], s_tp.at[j, k], r_tp.at[j, k], "tp", o)) for k, o in enumerate(mates)
         ]
+        for h in range(2):
+            direction = None
+            for part in pieces[h]:
+                piece = dot(left[i, 0:rows], part)
+                direction = piece if direction is None else direction + piece
+            step[i, :, h * half : (h + 1) * half] = direction
+        return trips
 
     def finish(j, i, trips):
         joint = pair[j, 0]
@@ -513,60 +570,73 @@
         step[i] = new_step
         copies[i, at.f] = (master[i] - step_size * new_step).astype(jnp.bfloat16)
 
-    def sems_of(group, j):
-        return [s.at[j] for s in group]
+    def grams(start):
+        yield start
+        if parts == 2:
+            find_gram(own)
+            gram_trip.append(go(send(left.at[own, gram], left.at[own, gram], s_gram.at[0], r_gram.at[0], "tp", mate)))
+        else:
+            find_gram(0)
+            find_gram(1)
+
+    def spread(pools, j, view, start, unit, also):
+        sems = banks(*pools, j, (0, 0), *gather_shapes(depth))
+        if depth == 4:
+            return line_gather(at, go, go_if, view, sems, start, unit, also)
+        return gather(at, go, view, sems, start, unit, also)
+
+    def drain():
+        old = started[:]
+        started.clear()
+
+        def wait():
+            for copy in old:
+                copy.wait_send()
+
+        return wait
 
     def stream(j, i, plan):
-        begin, scatter, ratio_time, direct_time, copy_time = plan
-        yield begin
+        factor_times, scatter_times, ratio_time, direct_time, copy_time = plan
+        yield from factor_gather(j, *factor_times)
+        yield scatter_times[0] - 0.01
         cot_loads[j].wait()
 
-        @pl.when(own != j)
-        def _():
-            mid_trip.wait_recv()
-
-        project(j, i)
-
-        def after_first():
-            if j == 0:
-                find_gram(own)
-                gram_trip.append(
-                    go(send(left.at[own, gram], left.at[own, gram], s_mate.at[1], r_mate.at[1], "tp", mate))
-                )
-                for copy in other_loads:
-                    copy.wait()
-
-        yield from reduce_scatter(j, i, scatter, after_first)
-        yield from gather(
-            at,
-            go,
+        yield from reduce_scatter(j, i, *scatter_times)
+        yield from spread(
+            (s_ratio, r_ratio),
+            j,
             lambda h, index: ratios.at[j, h, index],
-            sems_of(ratio_sems, j),
             ratio_time,
             low_rows * half * 4 / RATE,
+            [(15.0, drain())],
         )
         yield direct_time
 
-        @pl.when(own != j)
-        def _():
-            gram_trip[0].wait_recv()
+        if parts == 2:
+
+            @pl.when(own != j)
+            def _():
+                gram_trip[0].wait_recv()
 
         trips = direct(j, i)
         yield direct_time + 1.5
         finish(j, i, trips)
-        size = rows // 2
-        view = lambda h, index: copies.at[i, index, pl.ds(h * size, size)]
-        unit = size * cols * 2 / RATE
-        if depth == 4:
-            yield from line_gather(at, go, go_if, view, sems_of(copy_sems, j), copy_time, unit)
-        else:
-            yield from gather(at, go, view, sems_of(copy_sems, j), copy_time, unit)
+        block = rows // 2
+        yield from spread(
+            (s_pool, r_pool),
+            j,
+            lambda h, index: copies.at[i, index, pl.ds(h * block, block)],
+            copy_time,
+            block * cols * 2 / RATE,
+            [(5.5, drain())] if j else [],
+        )
 
     body = n * rows * cols * 2 * 5 / 16 / RATE
     merge(
         [
-            stream(0, 0, (0.0, 1.0, 15.0, 28.0, 31.0)),
-            stream(1, 1, (2.5, 8.0, 22.5, 38.0, 29.0 + body)),
+            stream(0, 0, ((0.0, 6.0, 7.2, 1.4), (12.0, 1.4, 12.8, 1.7, 3, 0.0), 28.5, 42.0, 45.0)),
+            stream(1, 1, ((3.0, 9.505, 13.5, 1.25), (14.0, 0.8, 17.0, 1.5, 0, 0.0), 37.5, 53.0, 44.0 + body)),
+            grams(27.5),
         ]
     )
     for copy in started:
@@ -630,6 +700,7 @@
     half = cols // 2
     shape = jax.ShapeDtypeStruct
     f32, bf16 = jnp.float32, jnp.bfloat16
+    shapes = [sum(functools.reduce(int.__mul__, both[k]) for both in gather_shapes(depth)) for k in range(2)]
     held = [
         VMEM((2, rows, cols), f32),
         VMEM((2, low_rows, cols), f32),
@@ -648,7 +719,7 @@
             VMEM((2, rows + 3 * rank, rank), bf16),
             VMEM((2, low_rows, cols), f32),
             VMEM((2, low_rows, cols), f32),
-            VMEM((n, rows, rank), bf16),
+            VMEM((2, n, rows, rank), bf16),
             VMEM((2, tokens, rank), f32),
             VMEM((2, 2, depth, 2, 2, low_rows, half), f32),
             VMEM((2, 2, depth, 2, low_rows, half), f32),
@@ -659,14 +730,16 @@
             VMEM((2, 2, n, low_rows, half), f32),
             VMEM((2, m, 8, 128), f32),
             DMA((11,)),
-            DMA((2,)),
-            DMA((2,)),
-            *[DMA((2, depth, 2))] * 6,
+            DMA((2, depth)),
+            DMA((2, depth)),
+            DMA((1,)),
+            DMA((1,)),
             DMA((2, m)),
             DMA((2, m)),
-            *gather_sems(n),
-            *gather_sems(n, 2),
-            *(line_sems(2) if depth == 4 else gather_sems(n, 2)),
+            DMA((2, 10 * depth)),
+            DMA((2, 10 * depth)),
+            DMA((2, shapes[0])),
+            DMA((2, shapes[1])),
         ],
         compiler_params=pltpu.CompilerParams(collective_id=1, has_side_effects=True, vmem_limit_bytes=50 * 2**20),
         name="update",

time: 135 us -> 129 us (0.956)
  Pallas kernels: 134 us -> 128 us
    pallas_call x1, Pallas kernels: 130 us -> 124 us  [local(): pl.pallas_call(functools.partial(main_kernel, n, m), out_shape=held, in_s...]
where the time goes in v3:
time: 129 us
  Pallas kernels  128 us (99%)
    pallas_call x1, Pallas kernels, local(): pl.pallas_call(functools.partial(main_kernel, n, m), out_shape=held, in_s...  124 us
    pallas_call x1, Pallas kernels, local(): pl.pallas_call(functools.partial(hand_kernel, depth), out_shape=[full, fu...  3.98 us

profile of v3, /device:TPU:0, one launch (start us, length us, event | category | flops | bytes accessed | tf_op | source)
XLA Modules:
  0.0 128.8 jit_solution(10675358203951982246)
XLA Ops:
  0.6 124.2 %update.1 = (f32[2,128,1024]{2,1,0:T(8,128)S(1)}, f32[2,16,1024]{2,1,0:T(8,128)S(1)}, f32[2,16,1024]{2,1,0:T(8,128)S(1)}, bf16[2,16,128,1024]{3,2,1,0:T(8,128)(2,1)S(1)}) custom-call(bf16[768,2048]{1,0:T(8,128)(2,1)} %refs_0_.1, bf16[768,1024]{1,0:T(8,128)(2,1)} %refs_1_.1, bf16[768,1024]{1,0:T(8,128)(2,1)} %refs_2_.1, f32[128,1024]{1,0:T(8,128)} %refs_3_.1, ...), custom_call_target="tpu_custom_call" | custom-call | tf_op jit(solution)/shard_map/update/pallas_call | solution.py:710
  124.8 4.0 %results.1 = (f32[128,1024]{1,0:T(8,128)}, f32[128,1024]{1,0:T(8,128)}, f32[16,1024]{1,0:T(8,128)}, f32[16,1024]{1,0:T(8,128)}, f32[16,1024]{1,0:T(8,128)}, /*in...) custom-call(f32[2,128,1024]{2,1,0:T(8,128)S(1)} %get-tuple-element.20.refs_0_, ...), custom_call_target="tpu_custom_call" | custom-call | tf_op jit(solution)/shard_map/results/pallas_call | solution.py:763

commit v4 on v3

--- a/solution.py
+++ b/solution.py
@@ -521,7 +521,7 @@
             last = max(when + HOP + 0.5 * unit, hold + 0.01 * k)
             events.append((last, functools.partial(stage_three, k)))
         yield from in_order(events)
-        yield last + HOP + unit
+        yield last + (HOP + unit if j else 0.3)
         for h in range(2):
             low = ready[j, h, depth - 1]
             for k in range(depth - 1):
@@ -634,9 +634,9 @@
     body = n * rows * cols * 2 * 5 / 16 / RATE
     merge(
         [
-            stream(0, 0, ((0.0, 6.0, 7.2, 1.4), (12.0, 1.4, 12.8, 1.7, 3, 0.0), 28.5, 42.0, 45.0)),
-            stream(1, 1, ((3.0, 9.505, 13.5, 1.25), (14.0, 0.8, 17.0, 1.5, 0, 0.0), 37.5, 53.0, 44.0 + body)),
-            grams(27.5),
+            stream(0, 0, ((0.0, 6.0, 7.2, 1.4), (12.0, 1.4, 12.8, 1.7, 3, 0.0), 26.0, 42.0, 45.0)),
+            stream(1, 1, ((3.0, 9.505, 13.5, 1.25), (14.9, 0.8, 19.5, 1.5, 0, 0.0), 35.5, 53.0, 46.0 + body)),
+            grams(26.2),
         ]
     )
     for copy in started:

time: 129 us -> 128 us (level)
  no operation moved by 1% of the time
where the time goes in v4:
time: 128 us
  Pallas kernels  127 us (99%)
    pallas_call x1, Pallas kernels, local(): pl.pallas_call(functools.partial(main_kernel, n, m), out_shape=held, in_s...  123 us
    pallas_call x1, Pallas kernels, local(): pl.pallas_call(functools.partial(hand_kernel, depth), out_shape=[full, fu...  3.98 us

profile of v4, /device:TPU:0, one launch (start us, length us, event | category | flops | bytes accessed | tf_op | source)
XLA Modules:
  0.0 127.6 jit_solution(12730892004802400410)
XLA Ops:
  0.6 123.0 %update.1 = (f32[2,128,1024]{2,1,0:T(8,128)S(1)}, f32[2,16,1024]{2,1,0:T(8,128)S(1)}, f32[2,16,1024]{2,1,0:T(8,128)S(1)}, bf16[2,16,128,1024]{3,2,1,0:T(8,128)(2,1)S(1)}) custom-call(bf16[768,2048]{1,0:T(8,128)(2,1)} %refs_0_.1, bf16[768,1024]{1,0:T(8,128)(2,1)} %refs_1_.1, bf16[768,1024]{1,0:T(8,128)(2,1)} %refs_2_.1, f32[128,1024]{1,0:T(8,128)} %refs_3_.1, ...), custom_call_target="tpu_custom_call" | custom-call | tf_op jit(solution)/shard_map/update/pallas_call | solution.py:710
  123.6 4.0 %results.1 = (f32[128,1024]{1,0:T(8,128)}, f32[128,1024]{1,0:T(8,128)}, f32[16,1024]{1,0:T(8,128)}, f32[16,1024]{1,0:T(8,128)}, f32[16,1024]{1,0:T(8,128)}, /*in...) custom-call(f32[2,128,1024]{2,1,0:T(8,128)S(1)} %get-tuple-element.20.refs_0_, ...), custom_call_target="tpu_custom_call" | custom-call | tf_op jit(solution)/shard_map/results/pallas_call | solution.py:763

commit v5 on v4

--- a/solution.py
+++ b/solution.py
@@ -635,7 +635,7 @@
     merge(
         [
             stream(0, 0, ((0.0, 6.0, 7.2, 1.4), (12.0, 1.4, 12.8, 1.7, 3, 0.0), 26.0, 42.0, 45.0)),
-            stream(1, 1, ((3.0, 9.505, 13.5, 1.25), (14.9, 0.8, 19.5, 1.5, 0, 0.0), 35.5, 53.0, 46.0 + body)),
+            stream(1, 1, ((1.2, 9.505, 13.5, 1.25), (14.9, 0.8, 19.5, 1.5, 0, 0.0), 35.5, 53.0, 46.0 + body)),
             grams(26.2),
         ]
     )

time: 128 us -> 127 us (level)
  no operation moved by 1% of the time
where the time goes in v5:
time: 127 us
  Pallas kernels  126 us (99%)
    pallas_call x1, Pallas kernels, local(): pl.pallas_call(functools.partial(main_kernel, n, m), out_shape=held, in_s...  122 us
    pallas_call x1, Pallas kernels, local(): pl.pallas_call(functools.partial(hand_kernel, depth), out_shape=[full, fu...  3.98 us

profile of v5, /device:TPU:0, one launch (start us, length us, event | category | flops | bytes accessed | tf_op | source)
XLA Modules:
  0.0 126.6 jit_solution(294123916351823771)
XLA Ops:
  0.6 122.0 %update.1 = (f32[2,128,1024]{2,1,0:T(8,128)S(1)}, f32[2,16,1024]{2,1,0:T(8,128)S(1)}, f32[2,16,1024]{2,1,0:T(8,128)S(1)}, bf16[2,16,128,1024]{3,2,1,0:T(8,128)(2,1)S(1)}) custom-call(bf16[768,2048]{1,0:T(8,128)(2,1)} %refs_0_.1, bf16[768,1024]{1,0:T(8,128)(2,1)} %refs_1_.1, bf16[768,1024]{1,0:T(8,128)(2,1)} %refs_2_.1, f32[128,1024]{1,0:T(8,128)} %refs_3_.1, ...), custom_call_target="tpu_custom_call" | custom-call | tf_op jit(solution)/shard_map/update/pallas_call | solution.py:710
  122.6 4.0 %results.1 = (f32[128,1024]{1,0:T(8,128)}, f32[128,1024]{1,0:T(8,128)}, f32[16,1024]{1,0:T(8,128)}, f32[16,1024]{1,0:T(8,128)}, f32[16,1024]{1,0:T(8,128)}, /*in...) custom-call(f32[2,128,1024]{2,1,0:T(8,128)S(1)} %get-tuple-element.20.refs_0_, ...), custom_call_target="tpu_custom_call" | custom-call | tf_op jit(solution)/shard_map/results/pallas_call | solution.py:763
